TPU v7x, 32 devices: a whole 2x2x4 slice. The times are simulated.
32 devices in a mesh: sp: 8 (over z, x), tp: 4 (over y, core).
Axes of the slice: x: 2, y: 2, z: 4, core: 2. Of those that a mesh axis runs over, the one named last changes fastest.
Arguments:
- pool_input: bfloat16 [2048, 256], P('sp', 'tp'), may hold values from -6 to 6
- pool_weight: bfloat16 [4, 64, 64], P('tp'), may hold values from -0.75 to 0.75
- pool_gain: bfloat16 [256], P('tp'), may hold values from 0.099609375 to 1.8984375
- out_weight: bfloat16 [256, 2048], P(None, 'tp'), may hold values from -0.375 to 0.375
- resid: bfloat16 [2048, 2048], P('sp', 'tp'), may hold values from -90 to 90
- norm_gain: bfloat16 [2048], P('tp'), may hold values from 0.099609375 to 1.8984375
- routes: int32 [2048, 2], P('sp'), may hold values from 0 to 7, all different within a row; in each aligned block of 256 rows (0 to 255, 256 to 511, ...) at most 128 rows name the same one
- route_weight: float32 [2048, 2], P('sp'), may hold values from 0.2 to 1
- expert_gate: bfloat16 [8, 2048, 4096], P('sp', None, 'tp'), may hold values from -0.375 to 0.375
- expert_up: bfloat16 [8, 2048, 4096], P('sp', None, 'tp'), may hold values from -0.375 to 0.375
- expert_down: bfloat16 [8, 4096, 2048], P('sp', 'tp'), may hold values from -0.0234375 to 0.0234375
Outputs:
- layer_out: bfloat16 [2048, 2048], P('sp', 'tp')
Inputs may be any that keep to these rules, and one draw needn't show every extreme that they name: `routes`: the 2 experts of a position differ. In each aligned block of 256 positions no expert is named by more than 128 assignments; some block reaches that bound.
All inputs are finite; a program needn't handle non-finite values.
Results may differ from a plain program's by a relative error of at most 0.0085.
Values may be sent and summed in bfloat16 or wider, within the bound.
A program may use at most 64 MiB of HBM per device.

v0:
```python
import functools

import jax
import jax.numpy as jnp
from jax import lax
from jax.experimental import pallas as pl
from jax.experimental.pallas import tpu as pltpu
from jax.sharding import PartitionSpec as P

GSIZE = 64
REACH = 16
TOPK = 2
CORES = 2
LANES = 128
CHUNK_ROWS = 256

GATE_LIMIT = 7.0
GATE_ALPHA = 1.702
NORM_EPS = 1e-05

F32 = jnp.float32
BF16 = jnp.bfloat16
MESH = pl.DeviceIdType.MESH


def dot(a, b):
    return jnp.dot(a, b, preferred_element_type=F32)


def layer_kernel(
    n, tp, cap,
    pool_ref, mix_ref, gain_ref, proj_ref, resid_ref, norm_ref, routes_ref, weight_ref, gate_hbm, up_hbm, down_hbm,
    out_ref,
    tail, halo, packed, squares, stream_ref, normed_ref,
    x, sent, wg, wu, wd, hidden, own, mine, pc_send, pc_recv, ys_send, ys_recv, res, ret, acc,
    w_sem, h_send, h_recv, m_send, m_recv, s_send, s_recv, a_send, a_recv, b_send, b_recv, c_send, c_recv, d_send, d_recv, e_send, e_recv, f_send, f_recv,
):
    ny = tp // CORES
    tok, feat = resid_ref.shape
    channels = pool_ref.shape[1]
    width = wg.shape[1]
    group = x.shape[0] // ys_send.shape[0]
    chunks = n // group
    rows = group * cap
    sp = lax.axis_index("sp")
    t = lax.axis_index("tp")
    y, core = t // CORES, t % CORES
    partner = y * CORES + (1 - core)

    loads = [
        pltpu.make_async_copy(gate_hbm.at[0], wg, w_sem.at[0]),
        pltpu.make_async_copy(up_hbm.at[0], wu, w_sem.at[1]),
        pltpu.make_async_copy(down_hbm.at[0], wd, w_sem.at[2]),
    ]
    for load in loads:
        load.start()

    barrier = pltpu.get_barrier_semaphore()
    peers = [(lax.rem(sp + d, n), t) for d in range(1, n)]
    peers += [(sp, lax.rem(t + k, tp)) for k in range(1, tp)]
    for peer in peers:
        pl.semaphore_signal(barrier, inc=1, device_id=peer, device_id_type=MESH)

    def cols(block):
        return pl.ds(pl.multiple_of(block * feat, LANES), feat)

    def remote(src, dst, send, recv, device):
        return pltpu.make_async_remote_copy(
            src_ref=src, dst_ref=dst, send_sem=send, recv_sem=recv, device_id=device, device_id_type=MESH
        )

    def copy_a(d):
        return remote(sent.at[d], x.at[d, :, cols(t)], a_send.at[d], a_recv.at[d], (lax.rem(sp + d, n), t))

    def copy_b(d, k):
        part = x.at[d, :, cols(t)]
        return remote(part, part, b_send.at[d, k], b_recv.at[d, k], (sp, lax.rem(y + k, ny) * CORES + core))

    def copy_c(d, k):
        part = x.at[d, :, cols(lax.rem(y + ny - k, ny) * CORES + core)]
        return remote(part, part, c_send.at[d, k], c_recv.at[d, k], (sp, partner))

    def copy_d(q):
        return remote(pc_send.at[q], pc_recv.at[q], d_send.at[q], d_recv.at[q], (sp, partner))

    def copy_e(q, k):
        return remote(
            ys_send.at[q, k], ys_recv.at[q, k], e_send.at[q, k], e_recv.at[q, k],
            (sp, lax.rem(y + k, ny) * CORES + core),
        )

    def copy_f(d):
        return remote(res.at[d], ret.at[d], f_send.at[d], f_recv.at[d], (lax.rem(sp + n - d, n), t))

    tail_copy = remote(tail, halo, h_send.at[0], h_recv.at[0], (lax.rem(sp + 1, n), t))

    def copy_m(k):
        return remote(packed.at[0], packed.at[k], m_send.at[k], m_recv.at[k], (sp, lax.rem(t + k, tp)))

    def copy_s(k):
        return remote(squares.at[0], squares.at[k], s_send.at[k], s_recv.at[k], (sp, lax.rem(t + k, tp)))

    tail[...] = jnp.zeros_like(tail)
    tail[:, :channels] = pool_ref[tok - REACH :, :].astype(F32)
    pl.semaphore_wait(barrier, len(peers))
    tail_copy.start()

    listed = jnp.concatenate(
        [routes_ref[...].astype(F32), weight_ref[...], jnp.zeros((8 - 2 * TOPK, tok), F32)], axis=0
    ).T
    routes = [listed[:, k : k + 1] for k in range(TOPK)]
    weights = [listed[:, TOPK + k : TOPK + k + 1] for k in range(TOPK)]
    lane = lax.broadcasted_iota(jnp.int32, (tok, LANES), 1).astype(F32)
    onehot = [jnp.where(route == lane, 1.0, 0.0) for route in routes]
    below = lax.broadcasted_iota(jnp.int32, (tok, tok), 1) < lax.broadcasted_iota(jnp.int32, (tok, tok), 0)
    earlier = dot(jnp.where(below, 1.0, 0.0).astype(BF16), sum(onehot).astype(BF16))
    keys = [
        routes[k] * float(cap) + jnp.sum(earlier * onehot[k], axis=1, keepdims=True) for k in range(TOPK)
    ]
    slot = lax.broadcasted_iota(jnp.int32, (tok, cap), 1)

    tail_copy.wait_recv()
    before = jnp.where(sp == 0, 0.0, halo[:, :channels])
    current = pool_ref[...].astype(F32)
    summed = jnp.concatenate([before, current], axis=0)
    groups = channels // GSIZE
    group_of = t * groups + lax.broadcasted_iota(jnp.int32, (1, channels), 1) // GSIZE
    level = lax.rem(group_of, 4)
    window, span = jnp.zeros((tok, channels), F32), jnp.zeros((1, channels), F32)
    for power in range(4):
        summed = summed + pltpu.roll(summed, 1 << power, 0)
        window = jnp.where(level == power, summed[REACH:], window)
        span = jnp.where(level == power, float(2 << power), span)
    place = (sp * tok + 1 + lax.broadcasted_iota(jnp.int32, (tok, channels), 0)).astype(F32)
    pooled = (window / jnp.minimum(place, span) - current).astype(BF16)
    mixed = jnp.concatenate(
        [dot(pooled[:, g * GSIZE : (g + 1) * GSIZE], mix_ref[g]) for g in range(groups)], axis=1
    )
    mixed = (mixed * gain_ref[...].astype(F32)).astype(BF16)
    folds = max(1, LANES // channels)
    short = tok // folds
    packed[0] = jnp.concatenate([mixed[i * short : (i + 1) * short] for i in range(folds)], axis=1)
    for k in range(1, tp):
        copy_m(k).start()

    def projected(k):
        block = packed[k]
        part = jnp.concatenate([block[:, i * channels : (i + 1) * channels] for i in range(folds)], axis=0)
        first = lax.rem(t + tp - k, tp) * channels
        return dot(part, proj_ref[pl.ds(pl.multiple_of(first, GSIZE), channels), :])

    acc[...] = resid_ref[...].astype(F32) + projected(0)
    for k in range(1, tp):
        copy_m(k).wait_recv()
        acc[...] += projected(k)
    stream_ref[...] = acc[...].astype(BF16)
    stream = stream_ref[...].astype(F32)
    power = jnp.sum(stream * stream, axis=1, keepdims=True)
    squares[0] = jnp.broadcast_to(power, (tok, LANES)).T[:8]
    for k in range(1, tp):
        copy_s(k).start()
    total = squares[0]
    for k in range(1, tp):
        copy_s(k).wait_recv()
        total = total + squares[k]
    scale = lax.rsqrt(total.T[:, :1] / x.shape[2] + NORM_EPS)
    normed_ref[...] = (stream_ref[...].astype(F32) * scale * norm_ref[...].astype(F32)).astype(BF16)

    def rows_for(expert):
        wanted = (slot + expert * cap).astype(F32)
        chosen = jnp.where(keys[0] == wanted, 1.0, 0.0)
        for key in keys[1:]:
            chosen = chosen + jnp.where(key == wanted, 1.0, 0.0)
        return lax.dot_general(
            chosen.astype(BF16), normed_ref[...], (((0,), (0,)), ((), ())), preferred_element_type=F32
        ).astype(BF16)

    for d in range(1, n):
        sent[d] = rows_for(lax.rem(sp + d, n))
        copy_a(d).start()
    x[0, :, cols(t)] = rows_for(sp)

    def forward_a(q):
        for d in range(q * group, (q + 1) * group):
            if d:
                copy_a(d).wait_recv()
            for k in range(1, ny):
                copy_b(d, k).start()
            copy_c(d, 0).start()

    def finish(q):
        total = mine[q]
        for k in range(1, ny):
            copy_e(q, k).wait_recv()
            total = total + ys_recv[q, k].astype(F32)
        total = total.astype(BF16)
        for i in range(group):
            d = q * group + i
            block = total[i * cap : (i + 1) * cap]
            if d:
                res[d] = block
                copy_f(d).start()
            else:
                ret[0] = block

    forward_a(0)
    for q in range(chunks):
        members = range(q * group, (q + 1) * group)
        if q + 1 < chunks:
            forward_a(q + 1)
        for d in members:
            for k in range(1, ny):
                copy_b(d, k).wait_recv()
                copy_c(d, k).start()
        for d in members:
            for k in range(ny):
                copy_c(d, k).wait_recv()
        if q == 0:
            loads[0].wait()
            loads[1].wait()

        step = min(width, 256)

        @pl.loop(0, width // step)
        def _(i):
            part = pl.ds(pl.multiple_of(i * step, LANES), step)
            chosen = x[q * group : (q + 1) * group].reshape(rows, x.shape[2])
            gate = jnp.minimum(dot(chosen, wg[:, part]), GATE_LIMIT)
            up = jnp.clip(dot(chosen, wu[:, part]), -GATE_LIMIT, GATE_LIMIT)
            hidden[:, part] = ((up + 1.0) * gate * jax.nn.sigmoid(GATE_ALPHA * gate)).astype(BF16)

        if q == 0:
            loads[2].wait()
        for k in range(ny):
            block = lax.rem(y + k, ny) * CORES + (1 - core)
            pc_send[q, :, k * feat : (k + 1) * feat] = dot(hidden[...], wd[:, cols(block)]).astype(BF16)
        copy_d(q).start()
        for k in range(ny):
            block = lax.rem(y + k, ny) * CORES + core
            own[:, k * feat : (k + 1) * feat] = dot(hidden[...], wd[:, cols(block)])
        if q:
            finish(q - 1)
        copy_d(q).wait_recv()
        for k in range(1, ny):
            part = slice(k * feat, (k + 1) * feat)
            ys_send[q, k] = (own[:, part] + pc_recv[q, :, part].astype(F32)).astype(BF16)
            copy_e(q, k).start()
        mine[q] = own[:, :feat] + pc_recv[q, :, :feat].astype(F32)
    finish(chunks - 1)

    heads = [weight.astype(BF16).astype(F32) for weight in weights]
    rests = [weights[k] - heads[k] for k in range(TOPK)]
    acc[...] = stream_ref[...].astype(F32)
    for d in range(n):
        if d:
            copy_f(d).wait_recv()
        wanted = (slot + lax.rem(sp + d, n) * cap).astype(F32)
        high = sum(jnp.where(keys[k] == wanted, heads[k], 0.0) for k in range(TOPK))
        low = sum(jnp.where(keys[k] == wanted, rests[k], 0.0) for k in range(TOPK))
        block = ret[d]
        acc[...] += dot(high.astype(BF16), block) + dot(low.astype(BF16), block)
    out_ref[...] = acc[...].astype(BF16)

    tail_copy.wait_send()
    for k in range(1, tp):
        copy_m(k).wait_send()
        copy_s(k).wait_send()
    for d in range(n):
        if d:
            copy_a(d).wait_send()
            copy_f(d).wait_send()
        for k in range(ny):
            if k:
                copy_b(d, k).wait_send()
            copy_c(d, k).wait_send()
    for q in range(chunks):
        copy_d(q).wait_send()
        for k in range(1, ny):
            copy_e(q, k).wait_send()


def on_device(
    pool_input, pool_weight, pool_gain, out_weight, resid, norm_gain,
    routes, route_weight, expert_gate, expert_up, expert_down,
):
    n, tp = lax.axis_size("sp"), lax.axis_size("tp")
    tok, feat = resid.shape
    channels = pool_input.shape[1]
    folds = max(1, LANES // channels)
    model, width = expert_gate.shape[1:]
    cap = 2 * tok * TOPK // n
    ny = tp // CORES
    group = min(n, max(1, CHUNK_ROWS // cap))
    chunks = n // group
    rows = group * cap
    sems = pltpu.SemaphoreType.DMA
    vmem = pl.BlockSpec(memory_space=pltpu.VMEM)
    hbm = pl.BlockSpec(memory_space=pl.ANY)
    return pl.pallas_call(
        functools.partial(layer_kernel, n, tp, cap),
        out_shape=jax.ShapeDtypeStruct((tok, feat), BF16),
        in_specs=[vmem] * 8 + [hbm] * 3,
        out_specs=vmem,
        scratch_shapes=[
            pltpu.VMEM((REACH, max(LANES, channels)), F32),
            pltpu.VMEM((REACH, max(LANES, channels)), F32),
            pltpu.VMEM((tp, tok // folds, folds * channels), BF16),
            pltpu.VMEM((tp, 8, tok), F32),
            pltpu.VMEM((tok, feat), BF16),
            pltpu.VMEM((tok, feat), BF16),
            pltpu.VMEM((n, cap, model), BF16),
            pltpu.VMEM((n, cap, feat), BF16),
            pltpu.VMEM((model, width), BF16),
            pltpu.VMEM((model, width), BF16),
            pltpu.VMEM((width, model), BF16),
            pltpu.VMEM((rows, width), BF16),
            pltpu.VMEM((rows, ny * feat), F32),
            pltpu.VMEM((chunks, rows, feat), F32),
            pltpu.VMEM((chunks, rows, ny * feat), BF16),
            pltpu.VMEM((chunks, rows, ny * feat), BF16),
            pltpu.VMEM((chunks, ny, rows, feat), BF16),
            pltpu.VMEM((chunks, ny, rows, feat), BF16),
            pltpu.VMEM((n, cap, feat), BF16),
            pltpu.VMEM((n, cap, feat), BF16),
            pltpu.VMEM((tok, feat), F32),
            sems((3,)),
            sems((1,)), sems((1,)),
            sems((tp,)), sems((tp,)),
            sems((tp,)), sems((tp,)),
            sems((n,)), sems((n,)),
            sems((n, ny)), sems((n, ny)),
            sems((n, ny)), sems((n, ny)),
            sems((chunks,)), sems((chunks,)),
            sems((chunks, ny)), sems((chunks, ny)),
            sems((n,)), sems((n,)),
        ],
        compiler_params=pltpu.CompilerParams(
            collective_id=0, has_side_effects=True, vmem_limit_bytes=56 * 1024 * 1024
        ),
    )(
        pool_input, pool_weight, pool_gain.reshape(1, -1), out_weight, resid, norm_gain.reshape(1, -1),
        routes.T, route_weight.T, expert_gate, expert_up, expert_down,
    )


def solution(mesh):
    in_specs = (
        P("sp", "tp"),
        P("tp", None, None),
        P("tp"),
        P(None, "tp"),
        P("sp", "tp"),
        P("tp"),
        P("sp", None),
        P("sp", None),
        P("sp", None, "tp"),
        P("sp", None, "tp"),
        P("sp", "tp", None),
    )
    return jax.shard_map(on_device, mesh=mesh, in_specs=in_specs, out_specs=P("sp", "tp"), check_vma=False)
```

profile of v0, /device:TPU:0, one launch (start us, length us, event | category | flops | bytes accessed | tf_op | source)
XLA Modules:
  0.0 96.5 jit_solution(12575461494604412282)
XLA Ops:
  0.0 1.3 %reshape.7.norm_ref = bf16[1,512]{1,0:T(2,128)(2,1)} reshape(bf16[512]{0:T(512)(128)(2,1)} %param.16) | data formatting | bytes 2048 | tf_op jit(solution)/shard_map/reshape | solution.py:341
  1.3 1.5 %copy.12.pool_ref = bf16[256,64]{1,0:T(8,128)(2,1)} copy(bf16[256,64]{0,1:T(8,128)(2,1)} %param.11) | data formatting | bytes 65536 | tf_op args[0]
  2.7 92.0 %shard_map.109 = bf16[256,512]{1,0:T(8,128)(2,1)} custom-call(bf16[256,64]{1,0:T(8,128)(2,1)} %copy.12.pool_ref, bf16[1,64,64]{2,1,0:T(8,128)(2,1)} %mix_ref.1, bf16[1,64]{1,0:T(2,128)(2,1)} %bitcast.5, bf16[256,512]{1,0:T(8,128)(2,1)} %proj_ref.1, bf16[256,512]{1,0:T(8,128)(2,1)} %resid_ref.1, bf16[1,512]{1,0:T(2,128)(2,1)} %reshape.7.norm_ref, ...), custom_call_target="tpu_custom_call" | custom-call | tf_op jit(solution)/shard_map/pallas_call | solution.py:299
  94.8 1.7 %copy.14 = bf16[256,512]{1,0:T(8,128)(2,1)} copy(bf16[256,512]{1,0:T(8,128)(2,1)} %shard_map.109) | data formatting | bytes 524288
where the time goes:
time: 96.7 us; the launch traced here: 96.5 us
  Pallas kernels  92 us (95%)
  local copies, waits for them, and re-layouts  4.41 us (5%)
    pallas_call x1, Pallas kernels, on_device(): pl.pallas_call(functools.partial(layer_kernel, n, tp, cap), out_shape=jax...  92 us
    unnamed x2, local copies, waits for them, and re-layouts  3.16 us

commit v1 on v0

v1 whole, which is shorter than its diff:
```python
import functools

import jax
import jax.numpy as jnp
from jax import lax
from jax.experimental import pallas as pl
from jax.experimental.pallas import tpu as pltpu
from jax.sharding import PartitionSpec as P

GSIZE = 64
REACH = 16
TOPK = 2
CORES = 2
LANES = 128
CHUNK_ROWS = 128
EARLY = 3

GATE_LIMIT = 7.0
GATE_ALPHA = 1.702
NORM_EPS = 1e-05

F32 = jnp.float32
BF16 = jnp.bfloat16
MESH = pl.DeviceIdType.MESH


def dot(a, b):
    return jnp.dot(a, b, preferred_element_type=F32)


def visiting_order(n):
    far = [(j / max(1, n // 2), d) for j, d in enumerate(range(n // 2, n)) if d > 1]
    near = [((j + 0.9) / max(1, n // 2 - 2), d) for j, d in enumerate(range(2, n // 2))]
    return list(range(min(n, 2))) + [d for _, d in sorted(far + near)]


def flipped(index, bits):
    bit = 1
    while bit <= bits:
        if bits & bit:
            index = index + bit * (1 - 2 * lax.rem(index // bit, 2))
        bit *= 2
    return index


def windows(summed, level):
    rows, channels = summed.shape
    window, span = jnp.zeros((rows - REACH, channels), F32), jnp.zeros((1, channels), F32)
    for power in range(4):
        summed = summed + pltpu.roll(summed, 1 << power, 0)
        window = jnp.where(level == power, summed[REACH:], window)
        span = jnp.where(level == power, float(2 << power), span)
    return window, span


def layer_kernel(
    n, tp, cap,
    pool_ref, mix_ref, gain_ref, proj_ref, resid_ref, norm_ref, routes_ref, weight_ref, gate_hbm, up_hbm, down_hbm,
    out_ref,
    edge, edges, packed, squares, stream_ref, normed_ref,
    x, sent, row_send, row_recv, wg, wu, wd, hidden, own, mine, pc_send, pc_recv, ys_send, ys_recv, res, ret, acc,
    w_sem, h_send, h_recv, m_send, m_recv, s_send, s_recv, g_send, g_recv, a_send, a_recv, b_send, b_recv, c_send, c_recv, d_send, d_recv, e_send, e_recv, f_send, f_recv,
):
    ny = tp // CORES
    tok, feat = resid_ref.shape
    channels = pool_ref.shape[0]
    model, width = wg.shape
    group = x.shape[0] // ys_send.shape[0]
    chunks = n // group
    rows = group * cap
    order = visiting_order(n)
    sp = lax.axis_index("sp")
    t = lax.axis_index("tp")
    y, core = t // CORES, t % CORES
    partner = y * CORES + (1 - core)
    other = [flipped(sp, d) for d in order]

    loads = [
        pltpu.make_async_copy(gate_hbm.at[0], wg, w_sem.at[0]),
        pltpu.make_async_copy(up_hbm.at[0], wu, w_sem.at[1]),
        pltpu.make_async_copy(down_hbm.at[0], wd, w_sem.at[2]),
    ]
    for load in loads:
        load.start()

    barrier = pltpu.get_barrier_semaphore()
    after, before = lax.rem(sp + 1, n), lax.rem(sp + n - 1, n)
    peers = [(other[i], t) for i in range(1, n)]
    peers += [(sp, lax.rem(t + k, tp)) for k in range(1, tp)]
    peers += [(s, lax.rem(t + k, tp)) for s in (after, before) for k in range(1, tp)]
    for peer in peers:
        pl.semaphore_signal(barrier, inc=1, device_id=peer, device_id_type=MESH)

    def cols(block):
        return pl.ds(pl.multiple_of(block * feat, LANES), feat)

    def remote(src, dst, send, recv, device):
        return pltpu.make_async_remote_copy(
            src_ref=src, dst_ref=dst, send_sem=send, recv_sem=recv, device_id=device, device_id_type=MESH
        )

    def copy_a(i):
        return remote(sent.at[i], x.at[i, :, cols(t)], a_send.at[i], a_recv.at[i], (other[i], t))

    def copy_g(i):
        return remote(row_send.at[i], row_recv.at[i], g_send.at[i], g_recv.at[i], (other[i], t))

    def copy_b(i, k):
        part = x.at[i, :, cols(t)]
        return remote(part, part, b_send.at[i, k], b_recv.at[i, k], (sp, lax.rem(y + k, ny) * CORES + core))

    def copy_c(i, k):
        part = x.at[i, :, cols(lax.rem(y + ny - k, ny) * CORES + core)]
        return remote(part, part, c_send.at[i, k], c_recv.at[i, k], (sp, partner))

    def copy_d(q):
        return remote(pc_send.at[q], pc_recv.at[q], d_send.at[q], d_recv.at[q], (sp, partner))

    def copy_e(q, k):
        return remote(
            ys_send.at[q, k], ys_recv.at[q, k], e_send.at[q, k], e_recv.at[q, k],
            (sp, lax.rem(y + k, ny) * CORES + core),
        )

    def copy_f(i):
        return remote(res.at[i], ret.at[i], f_send.at[i], f_recv.at[i], (other[i], t))

    def copy_h(k):
        return remote(edge, edges.at[k], h_send.at[k], h_recv.at[k], (after, lax.rem(t + k, tp)))

    def copy_m(k):
        return remote(packed.at[0], packed.at[k], m_send.at[k], m_recv.at[k], (sp, lax.rem(t + k, tp)))

    def copy_s(k):
        return remote(squares.at[0], squares.at[k], s_send.at[k], s_recv.at[k], (sp, lax.rem(t + k, tp)))

    with jax.named_scope("local"):
        current = pool_ref[...].astype(F32).T
        groups = channels // GSIZE
        group_of = t * groups + lax.broadcasted_iota(jnp.int32, (1, channels), 1) // GSIZE
        level = lax.rem(group_of, 4)
        blank = jnp.zeros((REACH, channels), F32)
        window, span = windows(jnp.concatenate([blank, current], axis=0), level)
        place = (sp * tok + 1 + lax.broadcasted_iota(jnp.int32, (tok, channels), 0)).astype(F32)
        pooled = (window / jnp.minimum(place, span) - current).astype(BF16)
        carried, _ = windows(jnp.concatenate([current[tok - REACH :], blank], axis=0), level)
        carried = (carried / span).astype(BF16)
        gain = gain_ref[...].astype(F32)

        def mix(values):
            parts = [dot(values[:, g * GSIZE : (g + 1) * GSIZE], mix_ref[g]) for g in range(groups)]
            return (jnp.concatenate(parts, axis=1) * gain).astype(BF16)

        mixed = mix(pooled)
        folds = max(1, LANES // channels)
        short = tok // folds
        packed[0] = jnp.concatenate([mixed[i * short : (i + 1) * short] for i in range(folds)], axis=1)
        edge[...] = jnp.concatenate([mix(carried)] * folds, axis=1)

        listed = jnp.concatenate(
            [routes_ref[...].astype(F32), weight_ref[...], jnp.zeros((8 - 2 * TOPK, tok), F32)], axis=0
        ).T
        routes = [listed[:, k : k + 1] for k in range(TOPK)]
        weights = [listed[:, TOPK + k : TOPK + k + 1] for k in range(TOPK)]
        lane = lax.broadcasted_iota(jnp.int32, (tok, LANES), 1).astype(F32)
        onehot = [jnp.where(route == lane, 1.0, 0.0) for route in routes]
        below = lax.broadcasted_iota(jnp.int32, (tok, tok), 1) < lax.broadcasted_iota(jnp.int32, (tok, tok), 0)
        earlier = dot(jnp.where(below, 1.0, 0.0).astype(BF16), sum(onehot).astype(BF16))
        keys = [
            routes[k] * float(cap) + jnp.sum(earlier * onehot[k], axis=1, keepdims=True) for k in range(TOPK)
        ]
        slot = lax.broadcasted_iota(jnp.int32, (tok, cap), 1)
        acc[...] = resid_ref[...].astype(F32)

    with jax.named_scope("barrier"):
        pl.semaphore_wait(barrier, len(peers))
    for k in range(1, tp):
        copy_m(k).start()

    @pl.when(sp < n - 1)
    def _():
        for k in range(tp):
            copy_h(k).start()

    def projected(block, k):
        first = lax.rem(t + tp - k, tp) * channels
        return dot(block, proj_ref[pl.ds(pl.multiple_of(first, GSIZE), channels), :])

    def unpacked(k):
        block = packed[k]
        return jnp.concatenate([block[:, i * channels : (i + 1) * channels] for i in range(folds)], axis=0)

    with jax.named_scope("proj"):
        acc[...] += projected(unpacked(0), 0)
        for k in range(1, tp):
            copy_m(k).wait_recv()
            acc[...] += projected(unpacked(k), k)

    with jax.named_scope("halo"):
        @pl.when(sp > 0)
        def _():
            for k in range(tp):
                copy_h(k).wait_recv()
                acc[:REACH] += projected(edges[k][:, :channels], k)

    with jax.named_scope("stream"):
        stream_ref[...] = acc[...].astype(BF16)
        stream = stream_ref[...].astype(F32)
        power = jnp.sum(stream * stream, axis=1, keepdims=True)
        squares[0] = jnp.broadcast_to(power, (tok, LANES)).T[:8]
        for k in range(1, tp):
            copy_s(k).start()
        normed_ref[...] = (stream * norm_ref[...].astype(F32)).astype(BF16)

    def chosen(i):
        wanted = (slot + other[i] * cap).astype(F32)
        return sum(jnp.where(key == wanted, 1.0, 0.0) for key in keys)

    def rows_for(i):
        return lax.dot_general(
            chosen(i).astype(BF16), normed_ref[...], (((0,), (0,)), ((), ())), preferred_element_type=F32
        ).astype(BF16)

    def arrive_a(i):
        if i:
            copy_a(i).wait_recv()
        for k in range(1, ny):
            copy_b(i, k).start()
        copy_c(i, 0).start()

    def arrive_b(i):
        for k in range(1, ny):
            copy_b(i, k).wait_recv()
            copy_c(i, k).start()

    def arrive_c(i):
        for k in range(ny):
            copy_c(i, k).wait_recv()

    def dispatch(first, last):
        for i in range(first, last):
            sent[i] = rows_for(i)
            copy_a(i).start()

    with jax.named_scope("dispatch"):
        x[0, :, cols(t)] = rows_for(0)
        arrive_a(0)
        early = min(n, 1 + EARLY)
        dispatch(1, early)

    with jax.named_scope("scales"):
        total = squares[0]
        for k in range(1, tp):
            copy_s(k).wait_recv()
            total = total + squares[k]
        scale = lax.rsqrt(total.T[:, :1] / model + NORM_EPS)
        for i in range(n):
            line = jnp.sum(chosen(i) * scale, axis=0, keepdims=True)
            if cap < LANES:
                line = jnp.concatenate([line, jnp.zeros((1, LANES - cap), F32)], axis=1)
            if i:
                row_send[i] = jnp.broadcast_to(line, row_send.shape[1:])
                copy_g(i).start()
            else:
                row_recv[0] = jnp.broadcast_to(line, row_send.shape[1:])
        dispatch(early, n)

    def finish(q):
        total = mine[q]
        for k in range(1, ny):
            copy_e(q, k).wait_recv()
            total = total + ys_recv[q, k].astype(F32)
        total = total.astype(BF16)
        for j in range(group):
            i = q * group + j
            block = total[j * cap : (j + 1) * cap]
            if i:
                res[i] = block
                copy_f(i).start()
            else:
                ret[0] = block

    def members(q):
        return range(q * group, (q + 1) * group) if q < chunks else ()

    with jax.named_scope("ahead"):
        for i in members(0):
            if i:
                arrive_a(i)
        for i in members(1):
            arrive_a(i)
        for i in members(0):
            arrive_b(i)
    for q in range(chunks):
        with jax.named_scope("wait_a"):
            for i in members(q + 2):
                arrive_a(i)
        with jax.named_scope("wait_b"):
            for i in members(q + 1):
                arrive_b(i)
        with jax.named_scope("wait_c"):
            for i in members(q):
                arrive_c(i)
                if i:
                    copy_g(i).wait_recv()
            scaled = jnp.concatenate([row_recv[i].T[:cap, :1] for i in members(q)], axis=0)
            if q == 0:
                loads[0].wait()
                loads[1].wait()

        with jax.named_scope("gateup"):
            step = min(width, 256)

            @pl.loop(0, width // step)
            def _(j):
                part = pl.ds(pl.multiple_of(j * step, LANES), step)
                block = x[q * group : (q + 1) * group].reshape(rows, model)
                gate = jnp.minimum(dot(block, wg[:, part]) * scaled, GATE_LIMIT)
                up = jnp.clip(dot(block, wu[:, part]) * scaled, -GATE_LIMIT, GATE_LIMIT)
                hidden[:, part] = ((up + 1.0) * gate * jax.nn.sigmoid(GATE_ALPHA * gate)).astype(BF16)

        with jax.named_scope("down"):
            if q == 0:
                loads[2].wait()
            for k in range(ny):
                block = lax.rem(y + k, ny) * CORES + (1 - core)
                pc_send[q, :, k * feat : (k + 1) * feat] = dot(hidden[...], wd[:, cols(block)]).astype(BF16)
            copy_d(q).start()
            for k in range(ny):
                block = lax.rem(y + k, ny) * CORES + core
                own[:, k * feat : (k + 1) * feat] = dot(hidden[...], wd[:, cols(block)])
        with jax.named_scope("finish"):
            if q:
                finish(q - 1)
        with jax.named_scope("wait_d"):
            copy_d(q).wait_recv()
            for k in range(1, ny):
                part = slice(k * feat, (k + 1) * feat)
                ys_send[q, k] = (own[:, part] + pc_recv[q, :, part].astype(F32)).astype(BF16)
                copy_e(q, k).start()
            mine[q] = own[:, :feat] + pc_recv[q, :, :feat].astype(F32)
    with jax.named_scope("finish"):
        finish(chunks - 1)

    heads = [weight.astype(BF16).astype(F32) for weight in weights]
    rests = [weights[k] - heads[k] for k in range(TOPK)]
    acc[...] = stream_ref[...].astype(F32)
    for i in range(n):
        with jax.named_scope("combine"):
            if i:
                copy_f(i).wait_recv()
            wanted = (slot + other[i] * cap).astype(F32)
            high = sum(jnp.where(keys[k] == wanted, heads[k], 0.0) for k in range(TOPK))
            low = sum(jnp.where(keys[k] == wanted, rests[k], 0.0) for k in range(TOPK))
            block = ret[i]
            acc[...] += dot(high.astype(BF16), block) + dot(low.astype(BF16), block)
    out_ref[...] = acc[...].astype(BF16)

    @pl.when(sp < n - 1)
    def _():
        for k in range(tp):
            copy_h(k).wait_send()

    for k in range(1, tp):
        copy_m(k).wait_send()
        copy_s(k).wait_send()
    for i in range(n):
        if i:
            copy_a(i).wait_send()
            copy_g(i).wait_send()
            copy_f(i).wait_send()
        for k in range(ny):
            if k:
                copy_b(i, k).wait_send()
            copy_c(i, k).wait_send()
    for q in range(chunks):
        copy_d(q).wait_send()
        for k in range(1, ny):
            copy_e(q, k).wait_send()


def on_device(
    pool_input, pool_weight, pool_gain, out_weight, resid, norm_gain,
    routes, route_weight, expert_gate, expert_up, expert_down,
):
    n, tp = lax.axis_size("sp"), lax.axis_size("tp")
    tok, feat = resid.shape
    channels = pool_input.shape[1]
    folds = max(1, LANES // channels)
    model, width = expert_gate.shape[1:]
    cap = 2 * tok * TOPK // n
    ny = tp // CORES
    group = min(n, max(1, CHUNK_ROWS // cap))
    chunks = n // group
    rows = group * cap
    sems = pltpu.SemaphoreType.DMA
    vmem = pl.BlockSpec(memory_space=pltpu.VMEM)
    hbm = pl.BlockSpec(memory_space=pl.ANY)
    return pl.pallas_call(
        functools.partial(layer_kernel, n, tp, cap),
        out_shape=jax.ShapeDtypeStruct((tok, feat), BF16),
        in_specs=[vmem] * 8 + [hbm] * 3,
        out_specs=vmem,
        scratch_shapes=[
            pltpu.VMEM((REACH, folds * channels), BF16),
            pltpu.VMEM((tp, REACH, folds * channels), BF16),
            pltpu.VMEM((tp, tok // folds, folds * channels), BF16),
            pltpu.VMEM((tp, 8, tok), F32),
            pltpu.VMEM((tok, feat), BF16),
            pltpu.VMEM((tok, feat), BF16),
            pltpu.VMEM((n, cap, model), BF16),
            pltpu.VMEM((n, cap, feat), BF16),
            pltpu.VMEM((n, 8, max(cap, LANES)), F32),
            pltpu.VMEM((n, 8, max(cap, LANES)), F32),
            pltpu.VMEM((model, width), BF16),
            pltpu.VMEM((model, width), BF16),
            pltpu.VMEM((width, model), BF16),
            pltpu.VMEM((rows, width), BF16),
            pltpu.VMEM((rows, ny * feat), F32),
            pltpu.VMEM((chunks, rows, feat), F32),
            pltpu.VMEM((chunks, rows, ny * feat), BF16),
            pltpu.VMEM((chunks, rows, ny * feat), BF16),
            pltpu.VMEM((chunks, ny, rows, feat), BF16),
            pltpu.VMEM((chunks, ny, rows, feat), BF16),
            pltpu.VMEM((n, cap, feat), BF16),
            pltpu.VMEM((n, cap, feat), BF16),
            pltpu.VMEM((tok, feat), F32),
            sems((3,)),
            sems((tp,)), sems((tp,)),
            sems((tp,)), sems((tp,)),
            sems((tp,)), sems((tp,)),
            sems((n,)), sems((n,)),
            sems((n,)), sems((n,)),
            sems((n, ny)), sems((n, ny)),
            sems((n, ny)), sems((n, ny)),
            sems((chunks,)), sems((chunks,)),
            sems((chunks, ny)), sems((chunks, ny)),
            sems((n,)), sems((n,)),
        ],
        compiler_params=pltpu.CompilerParams(
            collective_id=0, has_side_effects=True, vmem_limit_bytes=56 * 1024 * 1024
        ),
    )(
        pool_input.T, pool_weight, pool_gain.reshape(1, -1), out_weight, resid, norm_gain.reshape(1, -1),
        routes.T, route_weight.T, expert_gate, expert_up, expert_down,
    )


def solution(mesh):
    in_specs = (
        P("sp", "tp"),
        P("tp", None, None),
        P("tp"),
        P(None, "tp"),
        P("sp", "tp"),
        P("tp"),
        P("sp", None),
        P("sp", None),
        P("sp", None, "tp"),
        P("sp", None, "tp"),
        P("sp", "tp", None),
    )
    return jax.shard_map(on_device, mesh=mesh, in_specs=in_specs, out_specs=P("sp", "tp"), check_vma=False)
```

time: 96.7 us -> 82.5 us (0.85)
  Pallas kernels: 92 us -> 79.4 us
  local copies, waits for them, and re-layouts: 4.41 us -> 2.93 us
    pallas_call x1, Pallas kernels: 92 us -> 79.4 us  [on_device(): pl.pallas_call(functools.partial(layer_kernel, n, tp, cap), out_shape=jax...]
    unnamed x2 -> x1, local copies, waits for them, and re-layouts: 3.16 us -> 1.67 us
where the time goes in v1:
time: 82.5 us; the launch traced here: 82.4 us
  Pallas kernels  79.4 us (96%)
  local copies, waits for them, and re-layouts  2.93 us (4%)
    pallas_call x1, Pallas kernels, on_device(): pl.pallas_call(functools.partial(layer_kernel, n, tp, cap), out_shape=jax...  79.4 us
    unnamed x1, local copies, waits for them, and re-layouts  1.67 us

profile of v1, /device:TPU:0, one launch (start us, length us, event | category | flops | bytes accessed | tf_op | source)
XLA Modules:
  0.0 82.4 jit_solution(32763987368978063)
XLA Ops:
  0.0 1.3 %reshape.7.norm_ref = bf16[1,512]{1,0:T(2,128)(2,1)} reshape(bf16[512]{0:T(512)(128)(2,1)} %param.16) | data formatting | bytes 2048 | tf_op jit(solution)/shard_map/reshape | solution.py:444
  1.3 79.4 %shard_map.109 = bf16[256,512]{1,0:T(8,128)(2,1)} custom-call(bf16[64,256]{1,0:T(8,128)(2,1)} %bitcast.4, bf16[1,64,64]{2,1,0:T(8,128)(2,1)} %mix_ref.1, bf16[1,64]{1,0:T(2,128)(2,1)} %bitcast.7, bf16[256,512]{1,0:T(8,128)(2,1)} %proj_ref.1, bf16[256,512]{1,0:T(8,128)(2,1)} %resid_ref.1, bf16[1,512]{1,0:T(2,128)(2,1)} %reshape.7.norm_ref, s32[2,256]{1,0:T(2,128)} %bitcast.5, ...), custom_call_target="tpu_custom_call" | custom-call | tf_op jit(solution)/shard_map/pallas_call | solution.py:399
  80.7 1.7 %copy.13 = bf16[256,512]{1,0:T(8,128)(2,1)} copy(bf16[256,512]{1,0:T(8,128)(2,1)} %shard_map.109) | data formatting | bytes 524288

commit v2 on v1

--- a/solution.py
+++ b/solution.py
@@ -15,6 +15,23 @@
 CHUNK_ROWS = 128
 EARLY = 3
 
+VISITS = (0, 1, 4, 3, 5, 6, 7, 2)
+SENDS = (1, 2, 3, 4, 7, 5, 6)
+STEPS = (
+    ("relay", 0), ("gather", 1), ("gate_a", 0), ("gather", 2), ("gate_b", 0), ("down_theirs", 0), ("down_own", 0),
+    ("gather", 3), ("pair", 0), ("relay", 1), ("gate_a", 1), ("gate_b", 1), ("reduce", 0), ("relay", 2),
+    ("down_theirs", 1), ("down_own", 1), ("gate_a", 2), ("gather", 4), ("gate_b", 2), ("down_theirs", 2),
+    ("gather", 7), ("relay", 3), ("pair", 1), ("down_own", 2), ("relay", 4), ("gather", 5), ("gate_a", 3),
+    ("pair", 2), ("gate_b", 3), ("down_theirs", 3), ("reduce", 2), ("finish", 0), ("down_own", 3), ("gate_a", 4),
+    ("gather", 6), ("gate_b", 4), ("relay", 5), ("down_theirs", 4), ("down_own", 4), ("gate_a", 5), ("finish", 2),
+    ("pair", 4), ("reduce", 4), ("gate_b", 5), ("relay", 6), ("down_theirs", 5), ("pair", 3), ("reduce", 3),
+    ("down_own", 5), ("relay", 7), ("combine", 0), ("gate_a", 6), ("finish", 4), ("pair", 5), ("reduce", 5),
+    ("gate_b", 6), ("reduce", 1), ("down_theirs", 6), ("down_own", 6), ("pair", 6), ("finish", 3), ("gate_a", 7),
+    ("gate_b", 7), ("down_theirs", 7), ("reduce", 6), ("finish", 5), ("down_own", 7), ("finish", 1), ("pair", 7),
+    ("reduce", 7), ("finish", 6), ("combine", 3), ("combine", 4), ("combine", 1), ("finish", 7), ("combine", 2),
+    ("combine", 5), ("combine", 6), ("combine", 7),
+)
+
 GATE_LIMIT = 7.0
 GATE_ALPHA = 1.702
 NORM_EPS = 1e-05
@@ -28,10 +45,17 @@
     return jnp.dot(a, b, preferred_element_type=F32)
 
 
-def visiting_order(n):
-    far = [(j / max(1, n // 2), d) for j, d in enumerate(range(n // 2, n)) if d > 1]
-    near = [((j + 0.9) / max(1, n // 2 - 2), d) for j, d in enumerate(range(2, n // 2))]
-    return list(range(min(n, 2))) + [d for _, d in sorted(far + near)]
+def visiting_order(chunks, group):
+    order, sends, steps = VISITS, SENDS, STEPS
+    if chunks != len(VISITS):
+        order, sends, steps = range(chunks), range(1, chunks), [("relay", 0)]
+        for q in range(chunks):
+            steps += [(name, p) for name, p in (("gather", q + 1), ("relay", q + 1)) if p < chunks]
+            steps += [(name, q) for name in ("gate_a", "gate_b", "down_theirs", "down_own", "pair", "reduce")]
+        steps += [("finish", q) for q in range(chunks)] + [("combine", q) for q in range(chunks)]
+    offsets = [q * group + j for q in order for j in range(group)]
+    sending = [*range(1, group)] + [q * group + j for q in sends for j in range(group)]
+    return offsets, sending, steps
 
 
 def flipped(index, bits):
@@ -68,7 +92,8 @@
     group = x.shape[0] // ys_send.shape[0]
     chunks = n // group
     rows = group * cap
-    order = visiting_order(n)
+    order, sending, steps = visiting_order(chunks, group)
+    early = group - 1 + EARLY * group
     sp = lax.axis_index("sp")
     t = lax.axis_index("tp")
     y, core = t // CORES, t % CORES
@@ -210,7 +235,9 @@
         squares[0] = jnp.broadcast_to(power, (tok, LANES)).T[:8]
         for k in range(1, tp):
             copy_s(k).start()
-        normed_ref[...] = (stream * norm_ref[...].astype(F32)).astype(BF16)
+        scaling = norm_ref[...].astype(F32)
+        scaling = jnp.concatenate([scaling[i : i + 1] for i in range(feat // LANES)], axis=1)
+        normed_ref[...] = (stream * scaling).astype(BF16)
 
     def chosen(i):
         wanted = (slot + other[i] * cap).astype(F32)
@@ -238,15 +265,14 @@
             copy_c(i, k).wait_recv()
 
     def dispatch(first, last):
-        for i in range(first, last):
+        for i in sending[first:last]:
             sent[i] = rows_for(i)
             copy_a(i).start()
 
     with jax.named_scope("dispatch"):
         x[0, :, cols(t)] = rows_for(0)
         arrive_a(0)
-        early = min(n, 1 + EARLY)
-        dispatch(1, early)
+        dispatch(0, early)
 
     with jax.named_scope("scales"):
         total = squares[0]
@@ -265,6 +291,67 @@
                 row_recv[0] = jnp.broadcast_to(line, row_send.shape[1:])
         dispatch(early, n)
 
+    def members(q):
+        return range(q * group, (q + 1) * group) if q < chunks else ()
+
+    def gather(q):
+        for i in members(q):
+            arrive_a(i)
+
+    def relay(q):
+        for i in members(q):
+            arrive_b(i)
+
+    step = min(width, 256)
+
+    def gate_up(q, first, last):
+        scaled = jnp.concatenate([row_recv[i].T[:cap, :1] for i in members(q)], axis=0)
+
+        @pl.loop(first, last)
+        def _(j):
+            part = pl.ds(pl.multiple_of(j * step, LANES), step)
+            block = x[q * group : (q + 1) * group].reshape(rows, model)
+            gate = jnp.minimum(dot(block, wg[:, part]) * scaled, GATE_LIMIT)
+            up = jnp.clip(dot(block, wu[:, part]) * scaled, -GATE_LIMIT, GATE_LIMIT)
+            hidden[:, part] = ((up + 1.0) * gate * jax.nn.sigmoid(GATE_ALPHA * gate)).astype(BF16)
+
+    def gate_a(q):
+        for i in members(q):
+            arrive_c(i)
+            if i:
+                copy_g(i).wait_recv()
+        if q == 0:
+            loads[0].wait()
+            loads[1].wait()
+        gate_up(q, 0, width // step // 2)
+
+    def gate_b(q):
+        gate_up(q, width // step // 2, width // step)
+
+    def down_theirs(q):
+        if q == 0:
+            loads[2].wait()
+        for k in range(ny):
+            block = lax.rem(y + k, ny) * CORES + (1 - core)
+            pc_send[q, :, k * feat : (k + 1) * feat] = dot(hidden[...], wd[:, cols(block)]).astype(BF16)
+        copy_d(q).start()
+
+    def down_own(q):
+        for k in range(ny):
+            block = lax.rem(y + k, ny) * CORES + core
+            own[q % 2, :, k * feat : (k + 1) * feat] = dot(hidden[...], wd[:, cols(block)])
+
+    def pair(q):
+        copy_d(q).wait_recv()
+        for k in range(1, ny):
+            part = slice(k * feat, (k + 1) * feat)
+            ys_send[q, k] = (own[q % 2, :, part] + pc_recv[q, :, part].astype(F32)).astype(BF16)
+        mine[q] = own[q % 2, :, :feat] + pc_recv[q, :, :feat].astype(F32)
+
+    def reduce(q):
+        for k in range(1, ny):
+            copy_e(q, k).start()
+
     def finish(q):
         total = mine[q]
         for k in range(1, ny):
@@ -280,73 +367,11 @@
             else:
                 ret[0] = block
 
-    def members(q):
-        return range(q * group, (q + 1) * group) if q < chunks else ()
-
-    with jax.named_scope("ahead"):
-        for i in members(0):
-            if i:
-                arrive_a(i)
-        for i in members(1):
-            arrive_a(i)
-        for i in members(0):
-            arrive_b(i)
-    for q in range(chunks):
-        with jax.named_scope("wait_a"):
-            for i in members(q + 2):
-                arrive_a(i)
-        with jax.named_scope("wait_b"):
-            for i in members(q + 1):
-                arrive_b(i)
-        with jax.named_scope("wait_c"):
-            for i in members(q):
-                arrive_c(i)
-                if i:
-                    copy_g(i).wait_recv()
-            scaled = jnp.concatenate([row_recv[i].T[:cap, :1] for i in members(q)], axis=0)
-            if q == 0:
-                loads[0].wait()
-                loads[1].wait()
-
-        with jax.named_scope("gateup"):
-            step = min(width, 256)
-
-            @pl.loop(0, width // step)
-            def _(j):
-                part = pl.ds(pl.multiple_of(j * step, LANES), step)
-                block = x[q * group : (q + 1) * group].reshape(rows, model)
-                gate = jnp.minimum(dot(block, wg[:, part]) * scaled, GATE_LIMIT)
-                up = jnp.clip(dot(block, wu[:, part]) * scaled, -GATE_LIMIT, GATE_LIMIT)
-                hidden[:, part] = ((up + 1.0) * gate * jax.nn.sigmoid(GATE_ALPHA * gate)).astype(BF16)
-
-        with jax.named_scope("down"):
-            if q == 0:
-                loads[2].wait()
-            for k in range(ny):
-                block = lax.rem(y + k, ny) * CORES + (1 - core)
-                pc_send[q, :, k * feat : (k + 1) * feat] = dot(hidden[...], wd[:, cols(block)]).astype(BF16)
-            copy_d(q).start()
-            for k in range(ny):
-                block = lax.rem(y + k, ny) * CORES + core
-                own[:, k * feat : (k + 1) * feat] = dot(hidden[...], wd[:, cols(block)])
-        with jax.named_scope("finish"):
-            if q:
-                finish(q - 1)
-        with jax.named_scope("wait_d"):
-            copy_d(q).wait_recv()
-            for k in range(1, ny):
-                part = slice(k * feat, (k + 1) * feat)
-                ys_send[q, k] = (own[:, part] + pc_recv[q, :, part].astype(F32)).astype(BF16)
-                copy_e(q, k).start()
-            mine[q] = own[:, :feat] + pc_recv[q, :, :feat].astype(F32)
-    with jax.named_scope("finish"):
-        finish(chunks - 1)
-
     heads = [weight.astype(BF16).astype(F32) for weight in weights]
     rests = [weights[k] - heads[k] for k in range(TOPK)]
-    acc[...] = stream_ref[...].astype(F32)
-    for i in range(n):
-        with jax.named_scope("combine"):
+
+    def combine(q):
+        for i in members(q):
             if i:
                 copy_f(i).wait_recv()
             wanted = (slot + other[i] * cap).astype(F32)
@@ -354,7 +379,20 @@
             low = sum(jnp.where(keys[k] == wanted, rests[k], 0.0) for k in range(TOPK))
             block = ret[i]
             acc[...] += dot(high.astype(BF16), block) + dot(low.astype(BF16), block)
-    out_ref[...] = acc[...].astype(BF16)
+
+    acc[...] = stream_ref[...].astype(F32)
+    actions = dict(
+        gather=gather, relay=relay, gate_a=gate_a, gate_b=gate_b, down_theirs=down_theirs, down_own=down_own,
+        pair=pair, reduce=reduce, finish=finish, combine=combine,
+    )
+    for i in members(0):
+        if i:
+            arrive_a(i)
+    for name, q in steps:
+        with jax.named_scope(name + str(q)):
+            actions[name](q)
+    with jax.named_scope("out"):
+        out_ref[...] = acc[...].astype(BF16)
 
     @pl.when(sp < n - 1)
     def _():
@@ -398,7 +436,7 @@
     hbm = pl.BlockSpec(memory_space=pl.ANY)
     return pl.pallas_call(
         functools.partial(layer_kernel, n, tp, cap),
-        out_shape=jax.ShapeDtypeStruct((tok, feat), BF16),
+        out_shape=pltpu.VMEM((tok, feat), BF16),
         in_specs=[vmem] * 8 + [hbm] * 3,
         out_specs=vmem,
         scratch_shapes=[
@@ -416,7 +454,7 @@
             pltpu.VMEM((model, width), BF16),
             pltpu.VMEM((width, model), BF16),
             pltpu.VMEM((rows, width), BF16),
-            pltpu.VMEM((rows, ny * feat), F32),
+            pltpu.VMEM((2, rows, ny * feat), F32),
             pltpu.VMEM((chunks, rows, feat), F32),
             pltpu.VMEM((chunks, rows, ny * feat), BF16),
             pltpu.VMEM((chunks, rows, ny * feat), BF16),
@@ -441,7 +479,7 @@
             collective_id=0, has_side_effects=True, vmem_limit_bytes=56 * 1024 * 1024
         ),
     )(
-        pool_input.T, pool_weight, pool_gain.reshape(1, -1), out_weight, resid, norm_gain.reshape(1, -1),
+        pool_input.T, pool_weight, pool_gain.reshape(1, -1), out_weight, resid, norm_gain.reshape(-1, LANES),
         routes.T, route_weight.T, expert_gate, expert_up, expert_down,
     )
 

time: 82.5 us -> 70.8 us (0.86)
  Pallas kernels: 79.4 us -> 69.9 us
  local copies, waits for them, and re-layouts: 2.93 us -> 0.71 us
    pallas_call x1, Pallas kernels: 79.4 us -> 69.9 us  [on_device(): pl.pallas_call(functools.partial(layer_kernel, n, tp, cap), out_shape=plt...]
    reshape x1 -> x0, local copies, waits for them, and re-layouts: 1.26 us -> none  [on_device(): norm_gain.reshape(1, -1)]
    unnamed x1, local copies, waits for them, and re-layouts: 1.67 us -> 0.71 us
where the time goes in v2:
time: 70.8 us; the launch traced here: 70.7 us
  Pallas kernels  69.9 us (99%)
  local copies, waits for them, and re-layouts  0.71 us (1%)
    pallas_call x1, Pallas kernels, on_device(): pl.pallas_call(functools.partial(layer_kernel, n, tp, cap), out_shape=plt...  69.9 us

profile of v2, /device:TPU:0, one launch (start us, length us, event | category | flops | bytes accessed | tf_op | source)
XLA Modules:
  0.0 70.7 jit_solution(12973255525051257115)
XLA Ops:
  0.0 69.9 %shard_map.109 = bf16[256,512]{1,0:T(8,128)(2,1)S(1)} custom-call(bf16[64,256]{1,0:T(8,128)(2,1)} %bitcast.5, bf16[1,64,64]{2,1,0:T(8,128)(2,1)} %mix_ref.1, bf16[1,64]{1,0:T(2,128)(2,1)} %bitcast.9, bf16[256,512]{1,0:T(8,128)(2,1)} %proj_ref.1, bf16[256,512]{1,0:T(8,128)(2,1)} %resid_ref.1, bf16[4,128]{1,0:T(4,128)(2,1)} %bitcast.8, s32[2,256]{1,0:T(2,128)} %bitcast.6, ...), custom_call_target="tpu_custom_call" | custom-call | tf_op jit(solution)/shard_map/pallas_call | solution.py:437
  69.9 0.7 copy.13

commit v3 on v2

--- a/solution.py
+++ b/solution.py
@@ -79,11 +79,12 @@
 
 def layer_kernel(
     n, tp, cap,
-    pool_ref, mix_ref, gain_ref, proj_ref, resid_ref, norm_ref, routes_ref, weight_ref, gate_hbm, up_hbm, down_hbm,
+    pool_hbm, mix_hbm, gain_hbm, proj_hbm, resid_hbm, norm_hbm, routes_hbm, weight_hbm, gate_hbm, up_hbm, down_hbm,
     out_ref,
+    pool_ref, mix_ref, gain_ref, proj_ref, resid_ref, norm_ref, routes_ref, weight_ref,
     edge, edges, packed, squares, stream_ref, normed_ref,
     x, sent, row_send, row_recv, wg, wu, wd, hidden, own, mine, pc_send, pc_recv, ys_send, ys_recv, res, ret, acc,
-    w_sem, h_send, h_recv, m_send, m_recv, s_send, s_recv, g_send, g_recv, a_send, a_recv, b_send, b_recv, c_send, c_recv, d_send, d_recv, e_send, e_recv, f_send, f_recv,
+    i_sem, w_sem, h_send, h_recv, m_send, m_recv, s_send, s_recv, g_send, g_recv, a_send, a_recv, b_send, b_recv, c_send, c_recv, d_send, d_recv, e_send, e_recv, f_send, f_recv,
 ):
     ny = tp // CORES
     tok, feat = resid_ref.shape
@@ -105,8 +106,15 @@
         pltpu.make_async_copy(up_hbm.at[0], wu, w_sem.at[1]),
         pltpu.make_async_copy(down_hbm.at[0], wd, w_sem.at[2]),
     ]
-    for load in loads:
-        load.start()
+    fetches = [
+        pltpu.make_async_copy(source, target, i_sem.at[i])
+        for i, (source, target) in enumerate([
+            (pool_hbm, pool_ref), (mix_hbm, mix_ref), (gain_hbm, gain_ref), (routes_hbm, routes_ref),
+            (weight_hbm, weight_ref), (resid_hbm, resid_ref), (proj_hbm, proj_ref), (norm_hbm, norm_ref),
+        ])
+    ]
+    for fetch in fetches:
+        fetch.start()
 
     barrier = pltpu.get_barrier_semaphore()
     after, before = lax.rem(sp + 1, n), lax.rem(sp + n - 1, n)
@@ -115,6 +123,10 @@
     peers += [(s, lax.rem(t + k, tp)) for s in (after, before) for k in range(1, tp)]
     for peer in peers:
         pl.semaphore_signal(barrier, inc=1, device_id=peer, device_id_type=MESH)
+    for load in loads:
+        load.start()
+    for fetch in fetches:
+        fetch.wait()
 
     def cols(block):
         return pl.ds(pl.multiple_of(block * feat, LANES), feat)
@@ -434,12 +446,17 @@
     sems = pltpu.SemaphoreType.DMA
     vmem = pl.BlockSpec(memory_space=pltpu.VMEM)
     hbm = pl.BlockSpec(memory_space=pl.ANY)
+    operands = (
+        pool_input.T, pool_weight, pool_gain.reshape(1, -1), out_weight, resid, norm_gain.reshape(-1, LANES),
+        routes.T, route_weight.T, expert_gate, expert_up, expert_down,
+    )
     return pl.pallas_call(
         functools.partial(layer_kernel, n, tp, cap),
         out_shape=pltpu.VMEM((tok, feat), BF16),
-        in_specs=[vmem] * 8 + [hbm] * 3,
+        in_specs=[hbm] * len(operands),
         out_specs=vmem,
-        scratch_shapes=[
+        scratch_shapes=[pltpu.VMEM(operand.shape, operand.dtype) for operand in operands[:8]]
+        + [
             pltpu.VMEM((REACH, folds * channels), BF16),
             pltpu.VMEM((tp, REACH, folds * channels), BF16),
             pltpu.VMEM((tp, tok // folds, folds * channels), BF16),
@@ -463,6 +480,7 @@
             pltpu.VMEM((n, cap, feat), BF16),
             pltpu.VMEM((n, cap, feat), BF16),
             pltpu.VMEM((tok, feat), F32),
+            sems((8,)),
             sems((3,)),
             sems((tp,)), sems((tp,)),
             sems((tp,)), sems((tp,)),
@@ -478,10 +496,7 @@
         compiler_params=pltpu.CompilerParams(
             collective_id=0, has_side_effects=True, vmem_limit_bytes=56 * 1024 * 1024
         ),
-    )(
-        pool_input.T, pool_weight, pool_gain.reshape(1, -1), out_weight, resid, norm_gain.reshape(-1, LANES),
-        routes.T, route_weight.T, expert_gate, expert_up, expert_down,
-    )
+    )(*operands)
 
 
 def solution(mesh):

time: 70.8 us -> 69.9 us (0.987)
  Pallas kernels: 69.9 us -> 69 us
    pallas_call x1, Pallas kernels: 69.9 us -> 69 us  [on_device(): pl.pallas_call(functools.partial(layer_kernel, n, tp, cap), out_shape=plt...]
where the time goes in v3:
time: 69.9 us; the launch traced here: 69.7 us
  Pallas kernels  69 us (99%)
  local copies, waits for them, and re-layouts  0.71 us (1%)
    pallas_call x1, Pallas kernels, on_device(): pl.pallas_call(functools.partial(layer_kernel, n, tp, cap), out_shape=plt...  69 us

profile of v3, /device:TPU:0, one launch (start us, length us, event | category | flops | bytes accessed | tf_op | source)
XLA Modules:
  0.0 69.7 jit_solution(16440657495711193455)
XLA Ops:
  0.0 69.0 %shard_map.109 = bf16[256,512]{1,0:T(8,128)(2,1)S(1)} custom-call(bf16[64,256]{1,0:T(8,128)(2,1)} %bitcast.5, bf16[1,64,64]{2,1,0:T(8,128)(2,1)} %mix_hbm.1, bf16[1,64]{1,0:T(2,128)(2,1)} %bitcast.9, bf16[256,512]{1,0:T(8,128)(2,1)} %proj_hbm.1, bf16[256,512]{1,0:T(8,128)(2,1)} %resid_hbm.1, bf16[4,128]{1,0:T(4,128)(2,1)} %bitcast.8, s32[2,256]{1,0:T(2,128)} %bitcast.6, ...), custom_call_target="tpu_custom_call" | custom-call | tf_op jit(solution)/shard_map/pallas_call | solution.py:453
  69.0 0.7 %copy.13 = bf16[256,512]{1,0:T(8,128)(2,1)} copy(bf16[256,512]{1,0:T(8,128)(2,1)S(1)} %shard_map.109) | data formatting | bytes 524288
